TPU v7x, 32 devices: a whole 2x2x4 slice. The times are simulated.
32 devices in a mesh: sp: 8 (over z, y), tp: 4 (over x, core).
Axes of the slice: x: 2, y: 2, z: 4, core: 2. Of those that a mesh axis runs over, the one named last changes fastest.
Arguments:
- latents: bfloat16 [2560, 2048], P(('sp', 'tp')), may hold values from -12.5 to 12.5, as said below
- context: bfloat16 [1024, 2048], P('sp'), may hold values from -120 to 120, as said below
- cond_vec: float32 [2048], replicated, may hold values from -6 to 6
- ctx_vec: float32 [2048], replicated, may hold values from -6 to 6
- shift_w: bfloat16 [2048, 2048], P('sp', 'tp'), may hold values from -0.125 to 0.125
- scale_w: bfloat16 [2048, 2048], P('sp', 'tp'), may hold values from -0.125 to 0.125
- modgate_w: bfloat16 [2048, 2048], P('sp', 'tp'), may hold values from -0.125 to 0.125
- query_down_weight: bfloat16 [2048, 512], replicated, may hold values from -0.125 to 0.125
- latent_down_weight: bfloat16 [2048, 256], replicated, may hold values from -0.125 to 0.125
- rot_down: bfloat16 [2048, 32], replicated, may hold values from -0.125 to 0.125
- gate_w: bfloat16 [2048, 2048], P(None, 'tp'), may hold values from -0.125 to 0.125
- query_norm_gain: float32 [512], replicated, may hold values from 0.1 to 1.9
- latent_norm_gain: float32 [256], replicated, may hold values from 0.1 to 1.9
- query_plain_weight: bfloat16 [512, 2048], P(None, 'tp'), may hold values from -0.25 to 0.25
- query_rotary_weight: bfloat16 [512, 1024], P(None, 'tp'), may hold values from -0.25 to 0.25
- key_expand_weight: bfloat16 [256, 2048], P(None, 'tp'), may hold values from -0.375 to 0.375
- value_expand_weight: bfloat16 [256, 2048], P(None, 'tp'), may hold values from -0.375 to 0.375
- out_w: bfloat16 [2048, 2048], P('tp'), may hold values from -0.5 to 0.5
- norm_gain: float32 [2048], replicated, may hold values from 0.1 to 1.9
- norm_bias: float32 [2048], replicated, may hold values from -3 to 3
Outputs:
- mixed_out: bfloat16 [2560, 2048], P(('sp', 'tp'))
Inputs may be any that keep to these rules, and one draw needn't show every extreme that they name: `latents`: latent rows are noise plus three slow waves along the whole sequence. Most context rows have their own scales of 1 to 3; a few rows may be far larger.
All inputs are finite; a program needn't handle non-finite values.
Results may differ from a plain program's by a relative error of at most 0.024.
The roundings to bfloat16 on the way count: a program that leaves them out, or rounds other values in their place, can miss the bound.
Values may be sent and summed in bfloat16 or wider, within the bound.
A program may use at most 128 MiB of HBM per device.

v0:
```python
import jax
import jax.numpy as jnp
from jax import lax
from jax.sharding import PartitionSpec as P

PLAIN_HEAD_SIZE = 64
ROTARY_SIZE = 32
VALUE_HEAD_SIZE = 64
GRID_W = 64


rope_base = 10000.0
norm_floor = 1e-06
residual_weight = 2.0**0.5
score_floor = -1e30


def rms_scale(values, gain):
    return values * lax.rsqrt(jnp.mean(values * values, axis=-1, keepdims=True) + norm_floor) * gain


def rotate(values, positions):
    pair_count = ROTARY_SIZE // 4
    inverse = rope_base ** (-jnp.arange(pair_count, dtype=jnp.float32) / pair_count)
    grid_row = (positions // GRID_W).astype(jnp.float32)
    grid_col = (positions % GRID_W).astype(jnp.float32)
    angles = jnp.stack([grid_row[:, None] * inverse, grid_col[:, None] * inverse], axis=1)
    cosine = jnp.cos(angles)[:, None, :, None, :]
    sine_part = jnp.sin(angles)[:, None, :, None, :]
    shaped = values.reshape(values.shape[0], -1, 2, 2, pair_count)
    first_part = shaped[:, :, :, 0:1, :]
    second = shaped[:, :, :, 1:2, :]
    turned = jnp.concatenate(
        [first_part * cosine - second * sine_part, second * cosine + first_part * sine_part], axis=3
    )
    return turned.reshape(values.shape)


def project(rows, weight):
    return jnp.dot(rows, weight, preferred_element_type=jnp.float32)


def per_device(
    latents,
    context,
    cond_vec,
    ctx_vec,
    shift_w,
    scale_w,
    modgate_w,
    query_down_weight,
    latent_down_weight,
    rot_down,
    gate_w,
    query_norm_gain,
    latent_norm_gain,
    query_plain_weight,
    query_rotary_weight,
    key_expand_weight,
    value_expand_weight,
    out_w,
    norm_gain,
    norm_bias,
):
    width_tp = lax.axis_size("tp")
    block_rows = latents.shape[0]
    seq_rows = block_rows * width_tp
    slab_rows = shift_w.shape[0]
    sp_index = lax.axis_index("sp")
    cond_rows = jnp.stack([jax.nn.silu(cond_vec), jax.nn.silu(ctx_vec)]).astype(jnp.bfloat16)
    cond_here = lax.dynamic_slice_in_dim(cond_rows, sp_index * slab_rows, slab_rows, 1)
    shift_part = project(cond_here, shift_w)
    scale_part = project(cond_here, scale_w)
    gate_part = project(cond_here, modgate_w)
    columns = shift_w.shape[1]
    corner = (jnp.int32(0), lax.axis_index("tp") * columns)
    blank_rows = jnp.zeros((2, latents.shape[1]), jnp.float32)
    shift_vec, scale_vec, gate_vec = lax.psum(
        (
            lax.dynamic_update_slice(blank_rows, shift_part, corner),
            lax.dynamic_update_slice(blank_rows, scale_part, corner),
            lax.dynamic_update_slice(blank_rows, gate_part, corner),
        ),
        ("sp", "tp"),
    )
    latent_in = (latents.astype(jnp.float32) * (1.0 + scale_vec[0]) + shift_vec[0]).astype(
        jnp.bfloat16
    )
    context_in = (context.astype(jnp.float32) * (1.0 + scale_vec[1]) + shift_vec[1]).astype(
        jnp.bfloat16
    )
    heads_here = gate_w.shape[1] // VALUE_HEAD_SIZE
    rows_part = lax.all_gather(latent_in, "tp", axis=0, tiled=True)
    positions = sp_index * seq_rows + jnp.arange(rows_part.shape[0], dtype=jnp.int32)
    q_codes = rms_scale(project(rows_part, query_down_weight), query_norm_gain).astype(jnp.bfloat16)
    kv_codes = rms_scale(project(rows_part, latent_down_weight), latent_norm_gain).astype(
        jnp.bfloat16
    )
    key_rot = rotate(project(rows_part, rot_down), positions).astype(jnp.bfloat16)
    gate_act = project(rows_part, gate_w).astype(jnp.bfloat16)
    project_q_cont = project(q_codes, query_plain_weight).astype(jnp.bfloat16)
    project_q_rot = rotate(project(q_codes, query_rotary_weight), positions).astype(jnp.bfloat16)
    joined = jnp.concatenate([project_q_cont, project_q_rot, gate_act, kv_codes, key_rot], axis=1)
    edge_one = query_plain_weight.shape[1]
    edge_two = edge_one + query_rotary_weight.shape[1]
    edge_three = edge_two + gate_w.shape[1]
    edge_four = edge_three + latent_down_weight.shape[1]
    q_cont = joined[:, :edge_one].reshape(seq_rows, heads_here, PLAIN_HEAD_SIZE)
    q_rot = joined[:, edge_one:edge_two].reshape(seq_rows, heads_here, ROTARY_SIZE)
    gate_act = joined[:, edge_two:edge_three]
    kv_codes = joined[:, edge_three:edge_four]
    key_rot = joined[:, edge_four:]
    ctx_codes = rms_scale(project(context_in, latent_down_weight), latent_norm_gain).astype(
        jnp.bfloat16
    )
    ctx_rot = project(context_in, rot_down).astype(jnp.bfloat16)
    score_scale = (PLAIN_HEAD_SIZE + ROTARY_SIZE) ** (-0.5)

    def expand(codes):
        return (
            project(codes, key_expand_weight).astype(jnp.bfloat16),
            project(codes, value_expand_weight).astype(jnp.bfloat16),
        )

    def attend(running, key_block, value_block, rotary):
        row_top, row_total, weighted = running
        key_count = key_block.shape[0]
        scores = jnp.einsum(
            "qhd,khd->hqk",
            q_cont,
            key_block.reshape(key_count, heads_here, PLAIN_HEAD_SIZE),
            preferred_element_type=jnp.float32,
        )
        scores = (
            scores + jnp.einsum("qhd,kd->hqk", q_rot, rotary, preferred_element_type=jnp.float32)
        ) * score_scale
        new_top = jnp.maximum(row_top, jnp.max(scores, axis=-1))
        weights = jnp.exp(scores - new_top[:, :, None])
        factor = jnp.exp(row_top - new_top)
        row_total = row_total * factor + jnp.sum(weights, axis=-1)
        weighted = weighted * factor[:, :, None] + jnp.einsum(
            "hqk,khd->hqd",
            weights.astype(jnp.bfloat16),
            value_block.reshape(key_count, heads_here, VALUE_HEAD_SIZE),
            preferred_element_type=jnp.float32,
        )
        return (new_top, row_total, weighted)

    start_state = (
        jnp.full((heads_here, seq_rows), score_floor, jnp.float32),
        jnp.zeros((heads_here, seq_rows), jnp.float32),
        jnp.zeros((heads_here, seq_rows, VALUE_HEAD_SIZE), jnp.float32),
    )
    ctx_all_codes, ctx_all_rot = (
        lax.all_gather(ctx_codes, "sp", axis=0, tiled=True),
        lax.all_gather(ctx_rot, "sp", axis=0, tiled=True),
    )
    ctx_keys, ctx_values = expand(ctx_all_codes)
    running = attend(start_state, ctx_keys, ctx_values, ctx_all_rot)
    pieces = (
        lax.all_gather(kv_codes, "sp", axis=0, tiled=True),
        lax.all_gather(key_rot, "sp", axis=0, tiled=True),
    )
    total_rows = pieces[0].shape[0]
    unit_count = total_rows // seq_rows
    grouped = max(
        [1]
        + [
            divisor
            for divisor in range(1, unit_count + 1)
            if unit_count % divisor == 0 and divisor * seq_rows <= 1024
        ]
    )
    blocked = tuple(
        (
            member.reshape(unit_count // grouped, grouped * seq_rows, member.shape[1])
            for member in pieces
        )
    )

    def one_block(carried, members):
        key_block, value_block = expand(members[0])
        return (attend(carried, key_block, value_block, members[1]), None)

    result, unused = lax.scan(one_block, running, blocked)
    running = result
    row_top, row_total, weighted = running
    attended = jnp.transpose(weighted / row_total[:, :, None], (1, 0, 2)).reshape(
        seq_rows, heads_here * VALUE_HEAD_SIZE
    )
    gated = (attended * jax.nn.silu(gate_act.astype(jnp.float32))).astype(jnp.bfloat16)
    branch = lax.psum_scatter(
        project(gated, out_w).astype(jnp.bfloat16), "tp", scatter_dimension=0, tiled=True
    ).astype(jnp.float32)
    blended = residual_weight * latents.astype(jnp.float32) + gate_vec[0] * branch
    row_mean = jnp.mean(blended, axis=-1, keepdims=True)
    centred = blended - row_mean
    row_var = jnp.mean(centred * centred, axis=-1, keepdims=True)
    return (centred * lax.rsqrt(row_var + norm_floor) * norm_gain + norm_bias).astype(jnp.bfloat16)


def solution(mesh):
    in_specs = (
        P(("sp", "tp"), None),
        P("sp", None),
        P(),
        P(),
        P("sp", "tp"),
        P("sp", "tp"),
        P("sp", "tp"),
        P(),
        P(),
        P(),
        P(None, "tp"),
        P(),
        P(),
        P(None, "tp"),
        P(None, "tp"),
        P(None, "tp"),
        P(None, "tp"),
        P("tp", None),
        P(),
        P(),
    )
    out_specs = P(("sp", "tp"), None)
    return jax.shard_map(
        per_device, mesh=mesh, in_specs=in_specs, out_specs=out_specs, check_vma=False
    )
```

profile of v0, /device:TPU:0, one launch (start us, length us, event | category | flops | bytes accessed | tf_op | source)
XLA Modules:
  0.0 249.4 jit_solution(9773118889546091030)
XLA Ops:
  11.7 42.5 %all-reduce = (f32[2,2048]{1,0:T(2,128)S(1)}, f32[2,2048]{1,0:T(2,128)S(1)}, f32[2,2048]{1,0:T(2,128)S(1)}) all-reduce(f32[2,2048]{1,0:T(2,128)S(1)} %convolution_dynamic-update-slice_fusion, f32[2,2048]{1,0:T(2,128)S(1)} %convolution_dynamic-update-slice_fusion.1, ...), channel_id=1, replica_groups=mesh['sp'=8,'tp'=4] {'sp','tp'}, use_global_device_ids=true, to_apply=%region_2.3 | all-reduce | flops 12288 | bytes 98304 | tf_op jit(solution)/shard_map/psum | solution.py:78
  54.2 1.8 fusion.30
  57.4 26.1 %all_gather.17 = bf16[1024,32]{0,1:T(8,128)(2,1)S(1)} all-gather(bf16[128,32]{0,1:T(8,128)(2,1)S(1)} %convolution_convert_fusion.7), channel_id=1, replica_groups=mesh['sp'=8,'tp'=4] {'sp'}, dimensions={0}, use_global_device_ids=true | all-gather | bytes 73728 | tf_op jit(solution)/shard_map/all_gather | solution.py:156
  83.7 1.6 multiply_reduce_fusion.3
  85.4 31.5 %all_gather.16 = bf16[1024,256]{1,0:T(8,128)(2,1)S(1)} all-gather(bf16[128,256]{1,0:T(8,128)(2,1)S(1)} %multiply_convert_fusion.3), channel_id=1, replica_groups=mesh['sp'=8,'tp'=4] {'sp'}, dimensions={0}, use_global_device_ids=true | all-gather | bytes 589824 | tf_op jit(solution)/shard_map/all_gather | solution.py:155
  119.9 3.0 %multiply_reduce_fusion.1 = (f32[320]{0:T(512)S(1)}, f32[320,512]{1,0:T(8,128)S(1)}) fusion(bf16[320,2048]{1,0:T(8,128)(2,1)} %all-gather.4.cloned.1.call-done, bf16[2048,512]{1,0:T(8,128)(2,1)} %param.29), kind=kOutput, calls=%fused_computation.49 | convolution fusion | flops 671416000 | bytes 4064512 | tf_op jit(solution)/shard_map/dot_general | solution.py:40
  123.9 2.2 multiply_reduce_fusion.2
  127.0 1.8 fusion.58
  129.0 31.2 %all-gather = bf16[8,320,32]{1,2,0:T(8,128)(2,1)S(1)} all-gather(bf16[1,320,32]{1,2,0:T(8,128)(2,1)S(1)} %bitcast.115), channel_id=1, replica_groups=mesh['sp'=8,'tp'=4] {'sp'}, dimensions={0}, use_global_device_ids=true | all-gather | bytes 184320 | tf_op jit(solution)/shard_map/all_gather | solution.py:162
  162.8 1.8 fusion.56
  164.6 2.1 fusion.20
  166.7 2.2 fusion.24
  169.0 37.6 %while.14 = (s32[]{:T(128)}, f32[8,320]{1,0:T(8,128)S(1)}, f32[8,320]{1,0:T(8,128)S(1)}, f32[8,320,64]{1,2,0:T(8,128)S(1)}, bf16[4,640,256]{2,1,0:T(8,128)(2,1)}...) while((s32[]{:T(128)}, f32[8,320]{1,0:T(8,128)S(1)}, ...), condition=%wide.region_11.12_spmd, body=%wide.region_8.11_spmd.sunk | while | flops 872289280 | bytes 39624860 | solution.py:185
  171.6 2.2 fusion.112
  176.7 1.7 fusion.114
  181.0 2.2 fusion.112
  186.1 1.7 fusion.114
  190.3 2.2 fusion.112
  195.5 1.7 fusion.114
  199.7 2.2 fusion.112
  204.9 1.7 fusion.114
  209.0 4.8 %convolution_convert_fusion.2 = bf16[320,2048]{1,0:T(8,128)(2,1)} fusion(bf16[512,2048]{1,0:T(8,128)(2,1)S(1)} %copy-done, f32[320,512]{1,0:T(8,128)S(1)} %copy.40, bf16[320,2048]{1,0:T(8,128)(2,1)} %all-gather.4.cloned.1.call-done, bf16[2048,512]{1,0:T(8,128)(2,1)} %param.32), kind=kOutput, calls=%fused_computation.28 | convolution fusion | flops 1344143360 | bytes 7471104 | tf_op jit(solution)/shard_map/dot_general | solution.py:40
  213.8 24.7 %reduce-scatter.2.cloned.1.call-done = bf16[80,2048]{1,0:T(8,128)(2,1)} async-done(((bf16[320,2048]{1,0:T(8,128)(2,1)}), bf16[80,2048]{1,0:T(8,128)(2,1)}) %reduce-scatter.2.cloned.1.call-update) | async-done | bytes 327696 | tf_op jit(solution)/shard_map/reduce_scatter | solution.py:192
  241.0 1.9 add_convert_fusion.1
  (115 shorter events, 41.1 us)
Async XLA Ops:
  6.5 202.4 %copy-start = (bf16[512,2048]{1,0:T(8,128)(2,1)S(1)}, bf16[512,2048]{1,0:T(8,128)(2,1)}, u32[]{:S(2)}) copy-start(bf16[512,2048]{1,0:T(8,128)(2,1)} %param.39) | copy-start | bytes 6291460
  6.5 77.2 %copy-start.14 = (bf16[128,2048]{1,0:T(8,128)(2,1)S(1)}, bf16[128,2048]{1,0:T(8,128)(2,1)}, u32[]{:S(2)}) copy-start(bf16[128,2048]{1,0:T(8,128)(2,1)} %param.23) | copy-start | bytes 1572868
  6.5 78.8 %copy-start.13 = (f32[256]{0:T(256)S(1)}, f32[256]{0:T(256)}, u32[]{:S(2)}) copy-start(f32[256]{0:T(256)} %param.34) | copy-start | bytes 3076
  6.5 113.3 %all-gather.4.cloned.1.call-start = ((), (), s32[]{:S(2)}) async-start(), calls=%async_computation.1 | async-start | bytes 1638400 | tf_op jit(solution)/shard_map/all_gather | solution.py:93
  10.5 106.4 %copy-start.1 = (bf16[256,512]{1,0:T(8,128)(2,1)S(1)}, bf16[256,512]{1,0:T(8,128)(2,1)}, u32[]{:S(2)}) copy-start(bf16[256,512]{1,0:T(8,128)(2,1)} %param.37) | copy-start | bytes 786436
  56.0 113.0 %all-gather.6.cloned.1.call-start = ((), (), s32[]{:S(2)}) async-start(), calls=%async_computation.2 | async-start | bytes 1474560 | tf_op jit(solution)/shard_map/all_gather | solution.py:161
  56.1 62.3 %copy-start.2 = (bf16[256,512]{1,0:T(8,128)(2,1)S(1)}, bf16[256,512]{1,0:T(8,128)(2,1)}, u32[]{:S(2)}) copy-start(bf16[256,512]{1,0:T(8,128)(2,1)} %param.38) | copy-start | bytes 786436
  119.9 3.0 %copy-start.8 = (bf16[512,256]{1,0:T(8,128)(2,1)S(1)}, bf16[512,256]{1,0:T(8,128)(2,1)}, u32[]{:S(2)}) copy-start(bf16[512,256]{1,0:T(8,128)(2,1)} %param.36) | copy-start | bytes 786436
  119.9 3.0 %copy-start.12 = (f32[512]{0:T(512)S(1)}, f32[512]{0:T(512)}, u32[]{:S(2)}) copy-start(f32[512]{0:T(512)} %param.33) | copy-start | bytes 6148
  119.9 3.4 %copy-start.7 = (bf16[512,512]{1,0:T(8,128)(2,1)S(1)}, bf16[512,512]{1,0:T(8,128)(2,1)}, u32[]{:S(2)}) copy-start(bf16[512,512]{1,0:T(8,128)(2,1)} %param.35) | copy-start | bytes 1572868
  123.7 3.3 %copy-start.9 = (bf16[2048,32]{0,1:T(8,128)(2,1)S(1)}, bf16[2048,32]{0,1:T(8,128)(2,1)}, u32[]{:S(2)}) copy-start(bf16[2048,32]{0,1:T(8,128)(2,1)} %param.31) | copy-start | bytes 393220
  127.0 111.5 %reduce-scatter.2.cloned.1.call-start = ((), (), s32[]{:S(2)}) async-start(), calls=%async_computation.3 | async-start | bytes 1638400 | tf_op jit(solution)/shard_map/reduce_scatter | solution.py:192
  161.2 1.6 copy-start.5
  164.6 2.2 copy-start.6
  173.7 1.6 copy-start.3
  183.1 1.6 copy-start.3
  192.5 1.6 copy-start.3
  201.9 1.6 copy-start.3
  209.0 29.5 %copy-start.4 = (bf16[80,2048]{1,0:T(8,128)(2,1)S(1)}, bf16[80,2048]{1,0:T(8,128)(2,1)}, u32[]{:S(2)}) copy-start(bf16[80,2048]{1,0:T(8,128)(2,1)} %param.22) | copy-start | bytes 983044
  213.8 27.2 %copy-start.10 = (f32[2048]{0:T(1024)S(1)}, f32[2048]{0:T(1024)}, u32[]{:S(2)}) copy-start(f32[2048]{0:T(1024)} %param.41) | copy-start | bytes 24580
  213.8 27.2 %copy-start.11 = (f32[2048]{0:T(1024)S(1)}, f32[2048]{0:T(1024)}, u32[]{:S(2)}) copy-start(f32[2048]{0:T(1024)} %param.40) | copy-start | bytes 24580
Sparse Core Ops, SparseCore 0:
  56.1 17.9 all-gather.3
  127.1 40.2 all-gather.5
  213.9 24.5 reduce-scatter.1
where the time goes:
time: 251 us; the launch traced here: 249 us
  blocking collectives  131 us (52%)
  matrix products  58.6 us (23%)
  waiting for transfers between devices  24.7 us (10%)
  other arithmetic  18.4 us (7%)
  between operations  13.5 us (5%)
  local copies, waits for them, and re-layouts  2.64 us (1%)
    psum x1, blocking collectives, per_device(): lax.psum((lax.dynamic_update_slice(blank_rows, shift_part, corner), lax.d...  42.5 us
    dot_general x21, matrix products, project(): return jnp.dot(rows, weight, preferred_element_type=jnp.float32)  33.4 us
    all_gather x1, blocking collectives, per_device(): lax.all_gather(ctx_codes, 'sp', axis=0, tiled=True)  31.5 us
    all_gather x1, blocking collectives, per_device(): lax.all_gather(key_rot, 'sp', axis=0, tiled=True)  31.2 us
    all_gather x1, blocking collectives, per_device(): lax.all_gather(ctx_rot, 'sp', axis=0, tiled=True)  26.1 us
    reduce_scatter x1, waiting for transfers between devices, per_device(): lax.psum_scatter(project(gated, out_w).astype(jnp.bfloat16), 'tp', scatte...  24.7 us
    dot_general x5, matrix products, attend(): jnp.einsum('qhd,kd->hqk', q_rot, rotary, preferred_element_type=jnp.float32)  10.2 us
    dot_general x5, matrix products, attend(): jnp.einsum('hqk,khd->hqd', weights.astype(jnp.bfloat16), value_block.resh...  8.97 us
  transfers between devices with their start and end apart: 3, of which 1 were waited for; matrix products, arithmetic and copies ran while one was open for 7% of the time, Pallas kernels for 0%

commit v1 on v0

v1 whole, which is shorter than its diff:
```python
import math

import jax
import jax.numpy as jnp
from jax import lax
from jax.experimental import pallas as pl
from jax.experimental.pallas import tpu as pltpu
from jax.sharding import PartitionSpec as P

HEAD = 64
ROT = 32
GRID_W = 64
LANES = 128

rope_base = 10000.0
norm_floor = 1e-06
residual_weight = 2.0**0.5
F32 = jnp.float32
BF16 = jnp.bfloat16
MESH = pl.DeviceIdType.MESH


def dot(a, b):
    return jnp.dot(a, b, preferred_element_type=F32)


def ring_pos(sp, n):
    return jnp.where(sp % 2 == 0, sp // 2, n - 1 - sp // 2)


def ring_sp(r, n):
    return jnp.where(r < n // 2, 2 * r, 2 * (n - 1 - r) + 1)


def lane_iota(shape):
    return lax.broadcasted_iota(jnp.int32, shape, len(shape) - 1)


def make_kernel(n_sp, n_tp, rows, ctx_rows, width, heads):
    seq = rows * n_tp
    block = seq + ctx_rows
    half = block // 2
    n_x = n_tp // 2
    pairs = heads // 2
    q_groups = (heads * ROT) // LANES
    mod_cols = width // n_tp
    score_scale = (HEAD + ROT) ** (-0.5) * math.log2(math.e)
    last = n_sp // 2

    def kernel(
        lat_hbm, ctx_hbm, cond, shift_hbm, scale_hbm, mgate_hbm, qd_hbm, ld_hbm, rd_hbm, gw_hbm,
        q_gain, l_gain, qp_hbm, qr_hbm, ke_hbm, ve_hbm, ow_hbm, n_gain, n_bias,
        out,
        lat, ctx, w_shift, w_scale, w_mgate, qd, ld, rd, gw, qp, qr, ke, ve, ow,
        modbuf, vecs, X, cosb, sinb, codes, Q, gate, M, O, gated, pair_out, pair_in, x_out, x_in,
        own_acc,
        ld_sem, mod_s, mod_r, vec_s, vec_r, lat_s, lat_r, rel_s, rel_r,
        rr_s, rr_r, rl_s, rl_r, dr_s, dr_r, dl_s, dl_r, pr_s, pr_r, xs_s, xs_r,
    ):
        sp = lax.axis_index("sp")
        tp = lax.axis_index("tp")
        core = tp % 2
        xi = tp // 2
        partner = xi * 2 + (1 - core)
        r = ring_pos(sp, n_sp)

        loads = []

        def load(src, dst):
            c = pltpu.make_async_copy(src, dst, ld_sem.at[len(loads)])
            c.start()
            loads.append(c)
            return c

        l_mod = [load(shift_hbm, w_shift), load(scale_hbm, w_scale), load(mgate_hbm, w_mgate)]
        l_lat = load(lat_hbm, lat.at[tp])
        l_ctx = load(ctx_hbm, ctx)
        l_ld = load(ld_hbm, ld)
        l_rd = load(rd_hbm, rd)
        l_qd = load(qd_hbm, qd)
        l_gw = load(gw_hbm, gw)
        l_q = [load(qp_hbm, qp), load(qr_hbm, qr)]
        l_kv = [load(ke_hbm, ke), load(ve_hbm, ve)]
        l_ow = load(ow_hbm, ow)

        bar = pltpu.get_barrier_semaphore()
        for d in range(1, n_sp):
            pl.semaphore_signal(bar, inc=1, device_id=((sp + d) % n_sp, tp), device_id_type=MESH)
        for d in range(1, n_tp):
            pl.semaphore_signal(bar, inc=1, device_id=(sp, (tp + d) % n_tp), device_id_type=MESH)

        for c in l_mod:
            c.wait()
        modbuf[sp] = jnp.zeros((8, mod_cols), F32)
        cv = cond[...]
        for i, w in enumerate((w_shift, w_scale, w_mgate)):
            modbuf[sp, 2 * i : 2 * i + 2, :] = dot(cv, w[...])[0:2]
        pl.semaphore_wait(bar, n_sp + n_tp - 2)

        def remote(src, dst, s, rcv, dev):
            return pltpu.make_async_remote_copy(
                src_ref=src, dst_ref=dst, send_sem=s, recv_sem=rcv, device_id=dev, device_id_type=MESH
            )

        sends = []
        for d in range(1, n_sp):
            k = (sp + d) % n_sp
            c = remote(modbuf.at[sp], modbuf.at[sp], mod_s.at[d], mod_r.at[sp], (k, tp))
            c.start()
            sends.append(c)
        l_lat.wait()
        for d in range(1, n_x):
            k = ((xi + d) % n_x) * 2 + core
            c = remote(lat.at[tp], lat.at[tp], lat_s.at[d], lat_r.at[tp], (sp, k))
            c.start()
            sends.append(c)
        c = remote(lat.at[tp], lat.at[tp], lat_s.at[0], lat_r.at[tp], (sp, partner))
        c.start()
        sends.append(c)

        lane = lane_iota((seq, LANES))
        pos = sp * seq + lax.broadcasted_iota(jnp.int32, (seq, LANES), 0)
        pair_no = (lane % 8).astype(F32)
        inv = jnp.exp(pair_no * (-math.log(rope_base) / 8))
        grid_row = pos // GRID_W
        grid_col = pos - grid_row * GRID_W
        where_axis = jnp.where((lane % 32) < 16, grid_row, grid_col).astype(F32)
        ang = where_axis * inv
        cosb[...] = jnp.cos(ang)
        sinb[...] = jnp.where((lane % 16) < 8, -jnp.sin(ang), jnp.sin(ang))

        def rotate(v):
            ln = lane_iota(v.shape)
            sw = jnp.where((ln % 16) < 8, pltpu.roll(v, LANES - 8, 1), pltpu.roll(v, 8, 1))
            return v * cosb[...] + sw * sinb[...]

        for d in range(1, n_sp):
            k = (sp + d) % n_sp
            remote(modbuf.at[k], modbuf.at[k], mod_s.at[d], mod_r.at[k], (k, tp)).wait_recv()
        tot = modbuf[0]
        for k in range(1, n_sp):
            tot = tot + modbuf[k]
        vecs[tp] = tot
        for d in range(1, n_tp):
            k = (tp + d) % n_tp
            c = remote(vecs.at[tp], vecs.at[tp], vec_s.at[d], vec_r.at[tp], (sp, k))
            c.start()
            sends.append(c)
        for d in range(1, n_x):
            k = ((xi + d) % n_x) * 2 + core
            remote(lat.at[k], lat.at[k], lat_s.at[d], lat_r.at[k], (sp, k)).wait_recv()
            c = remote(lat.at[k], lat.at[k], rel_s.at[d], rel_r.at[k], (sp, partner))
            c.start()
            sends.append(c)
        for d in range(1, n_tp):
            k = (tp + d) % n_tp
            remote(vecs.at[k], vecs.at[k], vec_s.at[d], vec_r.at[k], (sp, k)).wait_recv()

        def vec_row(i):
            return jnp.concatenate([vecs[t, i : i + 1, :] for t in range(n_tp)], axis=1)

        shift0, shift1 = vec_row(0), vec_row(1)
        scale0, scale1 = 1.0 + vec_row(2), 1.0 + vec_row(3)
        l_ctx.wait()
        X[seq:block, :] = (ctx[...].astype(F32) * scale1 + shift1).astype(BF16)
        remote(lat.at[partner], lat.at[partner], lat_s.at[0], lat_r.at[partner], (sp, partner)).wait_recv()
        for d in range(1, n_x):
            k = ((xi + d) % n_x) * 2 + (1 - core)
            remote(lat.at[k], lat.at[k], rel_s.at[d], rel_r.at[k], (sp, partner)).wait_recv()
        for t in range(n_tp):
            X[t * rows : (t + 1) * rows, :] = (lat[t].astype(F32) * scale0 + shift0).astype(BF16)

        def rms(v, g):
            return v * lax.rsqrt(jnp.mean(v * v, axis=-1, keepdims=True) + norm_floor) * g

        l_ld.wait()
        l_rd.wait()
        lat_w = ld.shape[1]
        codes[r, :, 0:lat_w] = rms(dot(X[...], ld[...]), l_gain[...]).astype(BF16)
        kr = dot(X[...], rd[...])
        kr4 = jnp.concatenate([kr, kr, kr, kr], axis=1)
        codes[r, 0:seq, lat_w : lat_w + LANES] = rotate(kr4[0:seq]).astype(BF16)
        codes[r, seq:block, lat_w : lat_w + LANES] = kr4[seq:block].astype(BF16)

        right = ring_sp((r + 1) % n_sp, n_sp)
        left = ring_sp((r + n_sp - 1) % n_sp, n_sp)

        def part(owner, c):
            return codes.at[owner, pl.ds(pl.multiple_of(c * half, 16), half), :]

        def right_copy(owner, s):
            return remote(part(owner, core), part(owner, core), rr_s.at[s], rr_r.at[s], (right, tp))

        def left_copy(owner, s):
            return remote(part(owner, core), part(owner, core), rl_s.at[s], rl_r.at[s], (left, tp))

        def hand_right(owner, s, c):
            return remote(part(owner, c), part(owner, c), dr_s.at[s], dr_r.at[s], (sp, partner))

        def hand_left(owner, s, c):
            return remote(part(owner, c), part(owner, c), dl_s.at[s], dl_r.at[s], (sp, partner))

        right_copy(r, 1).start()
        left_copy(r, 1).start()

        l_qd.wait()
        qc = rms(dot(X[0:seq, :], qd[...]), q_gain[...]).astype(BF16)
        for c in l_q:
            c.wait()
        q_plain = dot(qc, qp[...]).astype(BF16)
        q_rotary = dot(qc, qr[...])
        lane_q = lane_iota((seq, LANES))
        for g in range(q_groups):
            turned = rotate(q_rotary[:, g * LANES : (g + 1) * LANES]).astype(BF16)
            for i in range(LANES // ROT):
                h = g * (LANES // ROT) + i
                lo = (h // 2) * LANES
                plain = q_plain[:, lo : lo + LANES]
                Q[h, :, 0:LANES] = jnp.where((lane_q // HEAD) == h % 2, plain, jnp.zeros_like(plain))
                Q[h, :, LANES : 2 * LANES] = jnp.where(
                    (lane_q // ROT) == i, turned, jnp.zeros_like(turned)
                )
        l_gw.wait()
        gate[...] = dot(X[0:seq, :], gw[...]).astype(BF16)

        for h in range(heads):
            M[h] = jnp.full((seq, LANES), -1e30, F32)
            O[h] = jnp.zeros((seq, LANES), F32)
        for c in l_kv:
            c.wait()

        def attend(owner):
            cd = codes[owner, :, 0:lat_w]
            rt = codes[owner, :, lat_w : lat_w + LANES]

            def one_pair(p, carry):
                cols = pl.ds(pl.multiple_of(p * LANES, LANES), LANES)
                kp = dot(cd, ke[:, cols]).astype(BF16)
                vp = dot(cd, ve[:, cols]).astype(BF16)
                kc = jnp.concatenate([kp, rt], axis=1)
                ln = lane_iota(vp.shape)
                for e in range(2):
                    h = 2 * p + e
                    s = lax.dot_general(
                        Q[h], kc, (((1,), (1,)), ((), ())), preferred_element_type=F32
                    )
                    top = M[h]
                    new = jnp.maximum(top, jnp.max(s, axis=1, keepdims=True))
                    M[h] = new
                    alpha = jnp.exp2((top - new) * score_scale)
                    w = jnp.exp2((s - new[:, 0:1]) * score_scale).astype(BF16)
                    v = jnp.where((ln // HEAD) == e, vp, jnp.ones_like(vp))
                    O[h] = O[h] * alpha + dot(w, v)
                return carry

            lax.fori_loop(0, pairs, one_pair, 0)

        attend(r)

        def step(s, carry):
            from_left = (r + n_sp - s) % n_sp
            from_right = (r + s) % n_sp
            right_copy(from_left, s).wait_recv()
            right_copy(from_left, s + 1).start()
            hand_right(from_left, s, core).start()
            left_copy(from_right, s).wait_recv()

            @pl.when(s < last - 1)
            def _():
                left_copy(from_right, s + 1).start()

            hand_left(from_right, s, core).start()
            hand_right(from_left, s, 1 - core).wait_recv()
            attend(from_left)
            hand_left(from_right, s, 1 - core).wait_recv()
            attend(from_right)
            return carry

        lax.fori_loop(1, last, step, 0)
        far = (r + n_sp - last) % n_sp
        right_copy(far, last).wait_recv()
        hand_right(far, last, core).start()
        hand_right(far, last, 1 - core).wait_recv()
        attend(far)

        ln2 = lane_iota((seq, LANES))
        for p in range(pairs):
            a, b = O[2 * p], O[2 * p + 1]
            num = jnp.where(ln2 < HEAD, a, b)
            den = pltpu.roll(jnp.where(ln2 < HEAD, b, a), HEAD, 1)
            gt = gate[:, p * LANES : (p + 1) * LANES].astype(F32)
            act = gt / (1.0 + jnp.exp(-gt))
            gated[:, p * LANES : (p + 1) * LANES] = (num / den * act).astype(BF16)

        l_ow.wait()

        def branch(t):
            return dot(gated[pl.ds(pl.multiple_of(t * rows, 16), rows), :], ow[...])

        for d in range(1, n_x + 1):
            x2 = (xi + d) % n_x
            pair_out[d - 1] = branch(x2 * 2 + 1 - core).astype(BF16)
            c = remote(pair_out.at[d - 1], pair_in.at[d - 1], pr_s.at[d - 1], pr_r.at[d - 1], (sp, partner))
            c.start()
            sends.append(c)
        for d in range(1, n_x + 1):
            x2 = (xi + d) % n_x
            mine = branch(x2 * 2 + core)
            remote(
                pair_out.at[d - 1], pair_in.at[d - 1], pr_s.at[d - 1], pr_r.at[d - 1], (sp, partner)
            ).wait_recv()
            mine = mine + pair_in[d - 1].astype(F32)
            if d < n_x:
                x_out[d - 1] = mine.astype(BF16)
                c = remote(x_out.at[d - 1], x_in.at[d - 1], xs_s.at[d - 1], xs_r.at[d - 1], (sp, x2 * 2 + core))
                c.start()
                sends.append(c)
            else:
                own_acc[...] = mine
        acc = own_acc[...]
        for d in range(1, n_x):
            x2 = (xi + d) % n_x
            remote(
                x_out.at[d - 1], x_in.at[d - 1], xs_s.at[d - 1], xs_r.at[d - 1], (sp, x2 * 2 + core)
            ).wait_recv()
            acc = acc + x_in[d - 1].astype(F32)
        blended = residual_weight * lat[tp].astype(F32) + vec_row(4) * acc
        centred = blended - jnp.mean(blended, axis=-1, keepdims=True)
        var = jnp.mean(centred * centred, axis=-1, keepdims=True)
        out[...] = (centred * lax.rsqrt(var + norm_floor) * n_gain[...] + n_bias[...]).astype(BF16)

        for c in sends:
            c.wait_send()
        right_copy(r, 1).wait_send()
        left_copy(r, 1).wait_send()

        def drain(s, carry):
            right_copy(r, s + 1).wait_send()
            hand_right(r, s, core).wait_send()
            hand_left(r, s, core).wait_send()

            @pl.when(s < last - 1)
            def _():
                left_copy(r, s + 1).wait_send()

            return carry

        lax.fori_loop(1, last, drain, 0)
        hand_right(r, last, core).wait_send()

    def scratch():
        bf = lambda *s: pltpu.VMEM(s, BF16)
        f3 = lambda *s: pltpu.VMEM(s, F32)
        sem = lambda k: pltpu.SemaphoreType.DMA((k,))
        slab = width // n_sp
        return bf, f3, sem, slab

    return kernel, scratch, seq, block


def per_device(
    latents, context, cond_vec, ctx_vec, shift_w, scale_w, modgate_w, query_down_weight,
    latent_down_weight, rot_down, gate_w, query_norm_gain, latent_norm_gain, query_plain_weight,
    query_rotary_weight, key_expand_weight, value_expand_weight, out_w, norm_gain, norm_bias,
):
    n_sp, n_tp = lax.axis_size("sp"), lax.axis_size("tp")
    rows, width = latents.shape
    ctx_rows = context.shape[0]
    hcols = gate_w.shape[1]
    heads = hcols // HEAD
    slab = shift_w.shape[0]
    kernel, scratch, seq, block = make_kernel(n_sp, n_tp, rows, ctx_rows, width, heads)
    bf, f3, sem, _ = scratch()
    cond_rows = jnp.stack([jax.nn.silu(cond_vec), jax.nn.silu(ctx_vec)]).astype(BF16)
    cond_here = lax.dynamic_slice_in_dim(cond_rows, lax.axis_index("sp") * slab, slab, 1)
    cond_here = jnp.pad(cond_here, ((0, 14), (0, 0)))
    n_x = n_tp // 2
    last = n_sp // 2
    lat_w = latent_down_weight.shape[1]
    any_spec = pl.BlockSpec(memory_space=pl.ANY)
    vm = pl.BlockSpec(memory_space=pltpu.VMEM)
    call = pl.pallas_call(
        kernel,
        out_shape=jax.ShapeDtypeStruct((rows, width), BF16),
        in_specs=[any_spec] * 2 + [vm] + [any_spec] * 7 + [vm] * 2 + [any_spec] * 5 + [vm] * 2,
        out_specs=vm,
        scratch_shapes=[
            bf(n_tp, rows, width), bf(*context.shape), bf(*shift_w.shape), bf(*scale_w.shape),
            bf(*modgate_w.shape), bf(*query_down_weight.shape), bf(*latent_down_weight.shape),
            bf(*rot_down.shape), bf(*gate_w.shape), bf(*query_plain_weight.shape),
            bf(*query_rotary_weight.shape), bf(*key_expand_weight.shape),
            bf(*value_expand_weight.shape), bf(*out_w.shape),
            f3(n_sp, 8, width // n_tp), f3(n_tp, 8, width // n_tp), bf(block, width),
            f3(seq, LANES), f3(seq, LANES), bf(n_sp, block, lat_w + LANES),
            bf(heads, seq, 2 * LANES), bf(seq, hcols), f3(heads, seq, LANES), f3(heads, seq, LANES),
            bf(seq, hcols), bf(n_x, rows, width), bf(n_x, rows, width), bf(n_x, rows, width),
            bf(n_x, rows, width), f3(rows, width),
            sem(16), sem(n_sp), sem(n_sp), sem(n_tp), sem(n_tp), sem(n_x), sem(n_tp), sem(n_x), sem(n_tp),
            sem(last + 1), sem(last + 1), sem(last + 1), sem(last + 1),
            sem(last + 1), sem(last + 1), sem(last + 1), sem(last + 1),
            sem(n_x), sem(n_x), sem(n_x), sem(n_x),
        ],
        compiler_params=pltpu.CompilerParams(
            collective_id=0, has_side_effects=True, vmem_limit_bytes=62 * 1024 * 1024
        ),
    )
    return call(
        latents, context, cond_here, shift_w, scale_w, modgate_w, query_down_weight,
        latent_down_weight, rot_down, gate_w, query_norm_gain.reshape(1, -1),
        latent_norm_gain.reshape(1, -1), query_plain_weight, query_rotary_weight,
        key_expand_weight, value_expand_weight, out_w, norm_gain.reshape(1, -1),
        norm_bias.reshape(1, -1),
    )


def solution(mesh):
    in_specs = (
        P(("sp", "tp"), None), P("sp", None), P(), P(), P("sp", "tp"), P("sp", "tp"), P("sp", "tp"),
        P(), P(), P(), P(None, "tp"), P(), P(), P(None, "tp"), P(None, "tp"), P(None, "tp"),
        P(None, "tp"), P("tp", None), P(), P(),
    )
    return jax.shard_map(
        per_device, mesh=mesh, in_specs=in_specs, out_specs=P(("sp", "tp"), None), check_vma=False
    )
```

time: 251 us -> 88.1 us (0.35)
  blocking collectives: 131 us -> 0 us
  Pallas kernels: 0 us -> 82 us
  matrix products: 58.6 us -> 0 us
  waiting for transfers between devices: 24.7 us -> 0 us
  other arithmetic: 18.4 us -> 1.5 us
  between operations: 13.5 us -> 0.03 us
    all_gather x3 -> x0, blocking collectives: 88.8 us -> none  [the longest x1 31.5 us: per_device(): lax.all_gather(ctx_codes, 'sp', axis=0, tiled=True)]
    pallas_call x0 -> x1, Pallas kernels: none -> 82 us  [per_device(): call(latents, context, cond_here, shift_w, scale_w, modgate_w, query_down...]
    dot_general x36 -> x0, matrix products: 58.6 us -> none  [the longest x21 33.4 us: project(): return jnp.dot(rows, weight, preferred_element_type=jnp.float32)]
    psum x1 -> x0, blocking collectives: 42.5 us -> none  [per_device(): lax.psum((lax.dynamic_update_slice(blank_rows, shift_part, corner), lax.d...]
    reduce_scatter x1 -> x0, waiting for transfers between devices: 24.7 us -> none  [per_device(): lax.psum_scatter(project(gated, out_w).astype(jnp.bfloat16), 'tp', scatte...]
    reduce_sum x7 -> x0, other arithmetic: 10.7 us -> none  [the longest x5 8.22 us: attend(): row_total = row_total * factor + jnp.sum(weights, axis=-1)]
    convert_element_type x5 -> x0, other arithmetic: 4.6 us -> none  [the longest x1 1.93 us: per_device(): (centred * lax.rsqrt(row_var + norm_floor) * norm_gain + norm_bias).astyp...]
    unnamed x28 -> x2, local copies, waits for them, and re-layouts: 0.06 us -> 3.62 us
  transfers between devices with their start and end apart: 3 -> 0, of which waited for: 1 -> 0; matrix products, arithmetic and copies ran while one was open for 7% -> 0% of each run, Pallas kernels for 0% -> 0%
where the time goes in v1:
time: 88.1 us; the launch traced here: 87.8 us
  Pallas kernels  82 us (93%)
  local copies, waits for them, and re-layouts  4.25 us (5%)
  other arithmetic  1.5 us (2%)
    pallas_call x1, Pallas kernels, per_device(): call(latents, context, cond_here, shift_w, scale_w, modgate_w, query_down...  82 us
    unnamed x2, local copies, waits for them, and re-layouts  3.62 us

profile of v1, /device:TPU:0, one launch (start us, length us, event | category | flops | bytes accessed | tf_op | source)
XLA Modules:
  0.0 87.8 jit_solution(13765186073857395033)
XLA Ops:
  0.0 0.7 multiply_convert_fusion.1
  0.7 0.7 multiply_convert_fusion
  1.4 0.1 fusion
  1.5 0.6 pad.4.cond
  2.1 1.9 %copy.21.rd_hbm = bf16[2048,32]{1,0:T(8,128)(2,1)} copy(bf16[2048,32]{0,1:T(8,128)(2,1)} %param.29) | data formatting | bytes 262144 | tf_op args[9]
  4.0 82.0 %shard_map.190 = bf16[80,2048]{1,0:T(8,128)(2,1)} custom-call(bf16[80,2048]{1,0:T(8,128)(2,1)} %lat_hbm.1, bf16[128,2048]{1,0:T(8,128)(2,1)} %ctx_hbm.1, bf16[16,256]{1,0:T(8,128)(2,1)} %pad.4.cond, bf16[256,512]{1,0:T(8,128)(2,1)} %shift_hbm.1, bf16[256,512]{1,0:T(8,128)(2,1)} %scale_hbm.1, bf16[256,512]{1,0:T(8,128)(2,1)} %mgate_hbm.1, ...), custom_call_target="tpu_custom_call" | custom-call | tf_op jit(solution)/shard_map/pallas_call | solution.py:407
  86.1 1.7 %copy.23 = bf16[80,2048]{1,0:T(8,128)(2,1)} copy(bf16[80,2048]{1,0:T(8,128)(2,1)} %shard_map.190) | data formatting | bytes 655360
  (2 shorter events, 0.0 us)

commit v2 on v1

v2 whole, which is shorter than its diff:
```python
import math

import jax
import jax.numpy as jnp
from jax import lax
from jax.experimental import pallas as pl
from jax.experimental.pallas import tpu as pltpu
from jax.sharding import PartitionSpec as P

HEAD = 64
ROT = 32
GRID_W = 64
LANES = 128

rope_base = 10000.0
norm_floor = 1e-06
residual_weight = 2.0**0.5
F32 = jnp.float32
BF16 = jnp.bfloat16
MESH = pl.DeviceIdType.MESH


def dot(a, b):
    return jnp.dot(a, b, preferred_element_type=F32)


def ring_pos(sp, n):
    return jnp.where(sp % 2 == 0, sp // 2, n - 1 - sp // 2)


def ring_sp(r, n):
    return jnp.where(r < n // 2, 2 * r, 2 * (n - 1 - r) + 1)


def lane_iota(shape):
    return lax.broadcasted_iota(jnp.int32, shape, len(shape) - 1)


def make_kernel(n_sp, n_tp, rows, ctx_rows, width, heads):
    seq = rows * n_tp
    block = seq + ctx_rows
    half = block // 2
    n_x = n_tp // 2
    pairs = heads // 2
    q_groups = (heads * ROT) // LANES
    mod_cols = width // n_tp
    score_scale = (HEAD + ROT) ** (-0.5) * math.log2(math.e)
    last = n_sp // 2

    def kernel(
        lat_hbm, ctx_hbm, cond0, cond1, shift_hbm, scale_hbm, mgate_hbm, qd_hbm, ld_hbm, rd_hbm, gw_hbm,
        q_gain, l_gain, qp_hbm, qr_hbm, ke_hbm, ve_hbm, ow_hbm, n_gain, n_bias,
        out,
        lat, ctx, w_shift, w_scale, w_mgate, qd, ld, rd, gw, qp, qr, kv, ow,
        modbuf, vecs, X, cosb, sinb, codes, Q, gate, M, O, gated, pair_out, pair_in, x_out, x_in,
        own_acc,
        ld_sem, mod_s, mod_r, vec_s, vec_r, lat_s, lat_r, rel_s, rel_r, own_s, own_r,
        rr_s, rr_r, rl_s, rl_r, dr_s, dr_r, dl_s, dl_r, pr_s, pr_r, xs_s, xs_r,
    ):
        sp = lax.axis_index("sp")
        tp = lax.axis_index("tp")
        core = tp % 2
        xi = tp // 2
        partner = xi * 2 + (1 - core)
        r = ring_pos(sp, n_sp)

        loads = []

        def load(src, dst):
            c = pltpu.make_async_copy(src, dst, ld_sem.at[len(loads)])
            c.start()
            loads.append(c)
            return c

        l_mod = [load(shift_hbm, w_shift), load(scale_hbm, w_scale), load(mgate_hbm, w_mgate)]
        l_lat = load(lat_hbm, lat.at[tp])
        l_ctx = load(ctx_hbm, ctx)
        l_ld = load(ld_hbm, ld)
        l_rd = load(rd_hbm, rd)
        l_qd = load(qd_hbm, qd)
        l_gw = load(gw_hbm, gw)
        l_q = [load(qp_hbm, qp), load(qr_hbm, qr)]
        l_kv = []
        for p in range(pairs):
            cols = pl.ds(p * LANES, LANES)
            l_kv.append(load(ke_hbm.at[:, cols], kv.at[p, :, pl.ds(0, LANES)]))
            l_kv.append(load(ve_hbm.at[:, cols], kv.at[p, :, pl.ds(LANES, LANES)]))
        l_ow = load(ow_hbm, ow)

        bar = pltpu.get_barrier_semaphore()
        for d in range(1, n_sp):
            pl.semaphore_signal(bar, inc=1, device_id=((sp + d) % n_sp, tp), device_id_type=MESH)
        for d in range(1, n_tp):
            pl.semaphore_signal(bar, inc=1, device_id=(sp, (tp + d) % n_tp), device_id_type=MESH)

        for c in l_mod:
            c.wait()
        modbuf[sp] = jnp.zeros((8, mod_cols), F32)
        slab = w_shift.shape[0]

        def slab_of(ref):
            if slab % LANES == 0:
                return ref[:, pl.ds(pl.multiple_of(sp * slab, LANES), slab)]
            per = LANES // slab
            window = ref[:, pl.ds(pl.multiple_of(sp // per * LANES, LANES), LANES)]
            v = window[:, 0:slab]
            for i in range(1, per):
                v = jnp.where(sp % per == i, window[:, i * slab : (i + 1) * slab], v)
            return v

        def silu(v):
            return v / (1.0 + jnp.exp(-v))

        row_no = lax.broadcasted_iota(jnp.int32, (16, slab), 0)
        cv = jnp.where(row_no == 0, silu(slab_of(cond0)), silu(slab_of(cond1))).astype(BF16)
        for i, w in enumerate((w_shift, w_scale, w_mgate)):
            modbuf[sp, 2 * i : 2 * i + 2, :] = dot(cv, w[...])[0:2]
        pl.semaphore_wait(bar, n_sp + n_tp - 2)

        def remote(src, dst, s, rcv, dev):
            return pltpu.make_async_remote_copy(
                src_ref=src, dst_ref=dst, send_sem=s, recv_sem=rcv, device_id=dev, device_id_type=MESH
            )

        sends = []
        for d in range(1, n_sp):
            k = (sp + d) % n_sp
            c = remote(modbuf.at[sp], modbuf.at[sp], mod_s.at[d], mod_r.at[sp], (k, tp))
            c.start()
            sends.append(c)
        l_lat.wait()
        early = rows // 2 // 16 * 16
        pieces = (pl.ds(0, early), pl.ds(early, rows - early))

        def lat_copy(owner, i, d, k):
            return remote(
                lat.at[owner, pieces[i]], lat.at[owner, pieces[i]], lat_s.at[2 * d + i],
                lat_r.at[2 * owner + i], (sp, k),
            )

        def relay_copy(owner, i, d):
            return remote(
                lat.at[owner, pieces[i]], lat.at[owner, pieces[i]], rel_s.at[2 * d + i],
                rel_r.at[2 * owner + i], (sp, partner),
            )

        def own_copy(owner):
            return remote(lat.at[owner], lat.at[owner], own_s.at[0], own_r.at[0], (sp, partner))

        def send_piece(i):
            for d in range(1, n_x):
                c = lat_copy(tp, i, d, ((xi + d) % n_x) * 2 + core)
                c.start()
                sends.append(c)

        send_piece(0)
        c = own_copy(tp)
        c.start()
        sends.append(c)

        lane = lane_iota((seq, LANES))
        pos = sp * seq + lax.broadcasted_iota(jnp.int32, (seq, LANES), 0)
        pair_no = (lane % 8).astype(F32)
        inv = jnp.exp(pair_no * (-math.log(rope_base) / 8))
        grid_row = pos // GRID_W
        grid_col = pos - grid_row * GRID_W
        where_axis = jnp.where((lane % 32) < 16, grid_row, grid_col).astype(F32)
        ang = where_axis * inv
        cosb[...] = jnp.cos(ang)
        sinb[...] = jnp.where((lane % 16) < 8, -jnp.sin(ang), jnp.sin(ang))

        def rotate(v, at):
            ln = lane_iota(v.shape)
            sw = jnp.where((ln % 16) < 8, pltpu.roll(v, LANES - 8, 1), pltpu.roll(v, 8, 1))
            return v * cosb[at, :] + sw * sinb[at, :]

        for d in range(1, n_sp):
            k = (sp + d) % n_sp
            remote(modbuf.at[k], modbuf.at[k], mod_s.at[d], mod_r.at[k], (k, tp)).wait_recv()
        tot = modbuf[0]
        for k in range(1, n_sp):
            tot = tot + modbuf[k]
        vecs[tp] = tot
        for d in range(1, n_tp):
            k = (tp + d) % n_tp
            c = remote(vecs.at[tp], vecs.at[tp], vec_s.at[d], vec_r.at[tp], (sp, k))
            c.start()
            sends.append(c)
        send_piece(1)
        for d in range(1, n_tp):
            k = (tp + d) % n_tp
            remote(vecs.at[k], vecs.at[k], vec_s.at[d], vec_r.at[k], (sp, k)).wait_recv()

        def vec_row(i):
            return jnp.concatenate([vecs[t, i : i + 1, :] for t in range(n_tp)], axis=1)

        shift0, shift1 = vec_row(0), vec_row(1)
        scale0, scale1 = 1.0 + vec_row(2), 1.0 + vec_row(3)
        chip_rows = 2 * rows
        lat_w = ld.shape[1]

        def rms(v, g):
            return v * lax.rsqrt(jnp.mean(v * v, axis=-1, keepdims=True) + norm_floor) * g

        def chip_at(x):
            return pl.ds(pl.multiple_of(x * chip_rows, 16), chip_rows)

        def encode(at, turn):
            v = X[at, :]
            codes[r, at, 0:lat_w] = rms(dot(v, ld[...]), l_gain[...]).astype(BF16)
            kr = lax.dot_general(v, rd[...], (((1,), (1,)), ((), ())), preferred_element_type=F32)
            kr = jnp.concatenate([kr] * (LANES // ROT), axis=1)
            codes[r, at, lat_w : lat_w + LANES] = (rotate(kr, at) if turn else kr).astype(BF16)

        def modulate(x):
            for c in range(2):
                t = 2 * x + c
                X[pl.ds(pl.multiple_of(t * rows, 8), rows), :] = (
                    lat[t].astype(F32) * scale0 + shift0
                ).astype(BF16)

        def queries(x):
            at = chip_at(x)
            v = X[at, :]
            qc = rms(dot(v, qd[...]), q_gain[...]).astype(BF16)
            q_plain = (dot(qc, qp[...]) * score_scale).astype(BF16)
            q_rotary = dot(qc, qr[...]) * score_scale
            lane_q = lane_iota((chip_rows, LANES))
            for g in range(q_groups):
                turned = rotate(q_rotary[:, g * LANES : (g + 1) * LANES], at).astype(BF16)
                for i in range(LANES // ROT):
                    h = g * (LANES // ROT) + i
                    lo = (h // 2) * LANES
                    plain = q_plain[:, lo : lo + LANES]
                    Q[h, at, 0:LANES] = jnp.where((lane_q // HEAD) == h % 2, plain, jnp.zeros_like(plain))
                    Q[h, at, LANES : 2 * LANES] = jnp.where(
                        (lane_q // ROT) == i, turned, jnp.zeros_like(turned)
                    )
            gate[at, :] = dot(v, gw[...]).astype(BF16)

        def relay(i):
            for d in range(1, n_x):
                k = ((xi + d) % n_x) * 2 + core
                lat_copy(k, i, d, k).wait_recv()
                c = relay_copy(k, i, d)
                c.start()
                sends.append(c)

        l_ctx.wait()
        X[seq:block, :] = (ctx[...].astype(F32) * scale1 + shift1).astype(BF16)
        own_copy(partner).wait_recv()
        modulate(xi)
        l_ld.wait()
        l_rd.wait()
        encode(pl.ds(seq, ctx_rows), False)
        encode(chip_at(xi), True)
        relay(0)
        l_qd.wait()
        for c in l_q:
            c.wait()
        l_gw.wait()
        queries(xi)
        relay(1)
        for d in range(1, n_x):
            x2 = (xi + d) % n_x
            for i in range(2):
                relay_copy(x2 * 2 + 1 - core, i, d).wait_recv()
            modulate(x2)
            encode(chip_at(x2), True)

        right = ring_sp((r + 1) % n_sp, n_sp)
        left = ring_sp((r + n_sp - 1) % n_sp, n_sp)

        def part(owner, c):
            return codes.at[owner, pl.ds(pl.multiple_of(c * half, 16), half), :]

        def right_copy(owner, s):
            return remote(part(owner, core), part(owner, core), rr_s.at[s], rr_r.at[s], (right, tp))

        def left_copy(owner, s):
            return remote(part(owner, core), part(owner, core), rl_s.at[s], rl_r.at[s], (left, tp))

        def hand_right(owner, s, c):
            return remote(part(owner, c), part(owner, c), dr_s.at[s], dr_r.at[s], (sp, partner))

        def hand_left(owner, s, c):
            return remote(part(owner, c), part(owner, c), dl_s.at[s], dl_r.at[s], (sp, partner))

        right_copy(r, 1).start()
        left_copy(r, 1).start()

        for d in range(1, n_x):
            queries((xi + d) % n_x)

        for h in range(heads):
            M[h] = jnp.full((seq, LANES), -1e30, F32)
            O[h] = jnp.zeros((seq, LANES), F32)
        for c in l_kv:
            c.wait()

        def attend(owners, at, first, stop):
            cds = [codes[w, :, 0:lat_w] for w in owners]
            rts = [codes[w, :, lat_w : lat_w + LANES] for w in owners]

            def wide(v):
                whole, rest = block // LANES, block % LANES
                return jnp.concatenate([v] * whole + ([v[:, :rest]] if rest else []), axis=1)

            def one_pair(p, carry):
                kvs = [dot(cd, kv[p]).astype(BF16) for cd in cds]
                kcs = [jnp.concatenate([x[:, 0:LANES], rt], axis=1) for x, rt in zip(kvs, rts)]
                ln = lane_iota((block, LANES))
                ss = [
                    [
                        lax.dot_general(
                            Q[2 * p + e, at, :], kc, (((1,), (1,)), ((), ())), preferred_element_type=F32
                        )
                        for kc in kcs
                    ]
                    for e in range(2)
                ]
                for e in range(2):
                    h = 2 * p + e
                    top = M[h, at, :]
                    new = top
                    for s in ss[e]:
                        new = jnp.maximum(new, jnp.max(s, axis=1, keepdims=True))
                    M[h, at, :] = new
                    acc = O[h, at, :] * jnp.exp2(top - new)
                    for s, x in zip(ss[e], kvs):
                        w = jnp.exp2(s - wide(new)).astype(BF16)
                        v = x[:, LANES : 2 * LANES]
                        v = jnp.where((ln // HEAD) == e, v, jnp.ones_like(v))
                        acc = acc + dot(w, v)
                    O[h, at, :] = acc
                return carry

            lax.fori_loop(first, stop, one_pair, 0, unroll=min(2, stop - first))

        everything = pl.ds(0, seq)
        attend((r,), everything, 0, pairs)

        def arrive(s):
            from_left = (r + n_sp - s) % n_sp
            from_right = (r + s) % n_sp
            right_copy(from_left, s).wait_recv()
            right_copy(from_left, s + 1).start()
            hand_right(from_left, s, core).start()
            left_copy(from_right, s).wait_recv()

            @pl.when(s < last - 1)
            def _():
                left_copy(from_right, s + 1).start()

            hand_left(from_right, s, core).start()

        def near_blocks(s):
            from_left = (r + n_sp - s) % n_sp
            from_right = (r + s) % n_sp
            hand_right(from_left, s, 1 - core).wait_recv()
            hand_left(from_right, s, 1 - core).wait_recv()
            return from_left, from_right

        middle = pairs // 2

        def step(s, carry):
            near = near_blocks(s)
            attend(near, everything, 0, middle)
            arrive(s + 1)
            attend(near, everything, middle, pairs)
            return carry

        def finish(x):
            at = chip_at(x)
            ln2 = lane_iota((chip_rows, LANES))
            for p in range(pairs):
                a, b = O[2 * p, at, :], O[2 * p + 1, at, :]
                num = jnp.where(ln2 < HEAD, a, b)
                den = pltpu.roll(jnp.where(ln2 < HEAD, b, a), HEAD, 1)
                gt = gate[at, p * LANES : (p + 1) * LANES].astype(F32)
                gated[at, p * LANES : (p + 1) * LANES] = (num / den * silu(gt)).astype(BF16)

        arrive(1)
        lax.fori_loop(1, last - 1, step, 0)
        near = near_blocks(last - 1)
        others = [(xi + d) % n_x for d in range(1, n_x)]
        for x2 in others:
            attend(near, chip_at(x2), 0, middle)
        far = (r + n_sp - last) % n_sp
        right_copy(far, last).wait_recv()
        hand_right(far, last, core).start()
        for x2 in others:
            attend(near, chip_at(x2), middle, pairs)
        hand_right(far, last, 1 - core).wait_recv()
        l_ow.wait()

        def branch(t):
            return dot(gated[pl.ds(pl.multiple_of(t * rows, 8), rows), :], ow[...])

        def pair_copy(d):
            return remote(
                pair_out.at[d - 1], pair_in.at[d - 1], pr_s.at[d - 1], pr_r.at[d - 1], (sp, partner)
            )

        def over_chip(d):
            x2 = (xi + d) % n_x
            finish(x2)
            pair_out[d - 1] = branch(x2 * 2 + 1 - core).astype(BF16)
            c = pair_copy(d)
            c.start()
            sends.append(c)
            mine = branch(x2 * 2 + core)
            pair_copy(d).wait_recv()
            return mine + pair_in[d - 1].astype(F32)

        for d in range(1, n_x):
            x2 = (xi + d) % n_x
            attend((far,), chip_at(x2), 0, pairs)
            x_out[d - 1] = over_chip(d).astype(BF16)
            c = remote(x_out.at[d - 1], x_in.at[d - 1], xs_s.at[d - 1], xs_r.at[d - 1], (sp, x2 * 2 + core))
            c.start()
            sends.append(c)
        attend(near + (far,), chip_at(xi), 0, pairs)
        own_acc[...] = over_chip(n_x)
        acc = own_acc[...]
        for d in range(1, n_x):
            x2 = (xi + d) % n_x
            remote(
                x_out.at[d - 1], x_in.at[d - 1], xs_s.at[d - 1], xs_r.at[d - 1], (sp, x2 * 2 + core)
            ).wait_recv()
            acc = acc + x_in[d - 1].astype(F32)
        blended = residual_weight * lat[tp].astype(F32) + vec_row(4) * acc
        centred = blended - jnp.mean(blended, axis=-1, keepdims=True)
        var = jnp.mean(centred * centred, axis=-1, keepdims=True)
        out[...] = (centred * lax.rsqrt(var + norm_floor) * n_gain[...] + n_bias[...]).astype(BF16)

        for c in sends:
            c.wait_send()
        right_copy(r, 1).wait_send()
        left_copy(r, 1).wait_send()

        def drain(s, carry):
            right_copy(r, s + 1).wait_send()
            hand_right(r, s, core).wait_send()
            hand_left(r, s, core).wait_send()

            @pl.when(s < last - 1)
            def _():
                left_copy(r, s + 1).wait_send()

            return carry

        lax.fori_loop(1, last, drain, 0)
        hand_right(r, last, core).wait_send()

    def scratch():
        bf = lambda *s: pltpu.VMEM(s, BF16)
        f3 = lambda *s: pltpu.VMEM(s, F32)
        sem = lambda k: pltpu.SemaphoreType.DMA((k,))
        slab = width // n_sp
        return bf, f3, sem, slab

    return kernel, scratch, seq, block


def per_device(
    latents, context, cond_vec, ctx_vec, shift_w, scale_w, modgate_w, query_down_weight,
    latent_down_weight, rot_down, gate_w, query_norm_gain, latent_norm_gain, query_plain_weight,
    query_rotary_weight, key_expand_weight, value_expand_weight, out_w, norm_gain, norm_bias,
):
    n_sp, n_tp = lax.axis_size("sp"), lax.axis_size("tp")
    rows, width = latents.shape
    ctx_rows = context.shape[0]
    hcols = gate_w.shape[1]
    heads = hcols // HEAD
    slab = shift_w.shape[0]
    kernel, scratch, seq, block = make_kernel(n_sp, n_tp, rows, ctx_rows, width, heads)
    bf, f3, sem, _ = scratch()
    n_x = n_tp // 2
    last = n_sp // 2
    lat_w = latent_down_weight.shape[1]
    any_spec = pl.BlockSpec(memory_space=pl.ANY)
    vm = pl.BlockSpec(memory_space=pltpu.VMEM)
    call = pl.pallas_call(
        kernel,
        out_shape=jax.ShapeDtypeStruct((rows, width), BF16),
        in_specs=[any_spec] * 2 + [vm] * 2 + [any_spec] * 7 + [vm] * 2 + [any_spec] * 5 + [vm] * 2,
        out_specs=vm,
        scratch_shapes=[
            bf(n_tp, rows, width), bf(*context.shape), bf(*shift_w.shape), bf(*scale_w.shape),
            bf(*modgate_w.shape), bf(*query_down_weight.shape), bf(*latent_down_weight.shape),
            bf(*rot_down.shape[::-1]), bf(*gate_w.shape), bf(*query_plain_weight.shape),
            bf(*query_rotary_weight.shape), bf(heads // 2, lat_w, 2 * LANES), bf(*out_w.shape),
            f3(n_sp, 8, width // n_tp), f3(n_tp, 8, width // n_tp), bf(block, width),
            f3(seq, LANES), f3(seq, LANES), bf(n_sp, block, lat_w + LANES),
            bf(heads, seq, 2 * LANES), bf(seq, hcols), f3(heads, seq, LANES), f3(heads, seq, LANES),
            bf(seq, hcols), bf(n_x, rows, width), bf(n_x, rows, width), bf(n_x, rows, width),
            bf(n_x, rows, width), f3(rows, width),
            sem(12 + heads), sem(n_sp), sem(n_sp), sem(n_tp), sem(n_tp), sem(2 * n_x), sem(2 * n_tp), sem(2 * n_x), sem(2 * n_tp), sem(1), sem(1),
            sem(last + 1), sem(last + 1), sem(last + 1), sem(last + 1),
            sem(last + 1), sem(last + 1), sem(last + 1), sem(last + 1),
            sem(n_x), sem(n_x), sem(n_x), sem(n_x),
        ],
        compiler_params=pltpu.CompilerParams(
            collective_id=0, has_side_effects=True, vmem_limit_bytes=62 * 1024 * 1024
        ),
    )
    return call(
        latents, context, cond_vec.reshape(1, -1), ctx_vec.reshape(1, -1), shift_w, scale_w, modgate_w, query_down_weight,
        latent_down_weight, rot_down.T, gate_w, query_norm_gain.reshape(1, -1),
        latent_norm_gain.reshape(1, -1), query_plain_weight, query_rotary_weight,
        key_expand_weight, value_expand_weight, out_w, norm_gain.reshape(1, -1),
        norm_bias.reshape(1, -1),
    )


def solution(mesh):
    in_specs = (
        P(("sp", "tp"), None), P("sp", None), P(), P(), P("sp", "tp"), P("sp", "tp"), P("sp", "tp"),
        P(), P(), P(), P(None, "tp"), P(), P(), P(None, "tp"), P(None, "tp"), P(None, "tp"),
        P(None, "tp"), P("tp", None), P(), P(),
    )
    return jax.shard_map(
        per_device, mesh=mesh, in_specs=in_specs, out_specs=P(("sp", "tp"), None), check_vma=False
    )
```

time: 88.1 us -> 59.5 us (0.68)
  Pallas kernels: 82 us -> 57.5 us
  local copies, waits for them, and re-layouts: 4.25 us -> 1.72 us
  other arithmetic: 1.5 us -> 0 us
    pallas_call x1, Pallas kernels: 82 us -> 57.5 us  [per_device(): call(latents, context, cond_vec.reshape(1, -1), ctx_vec.reshape(1, -1), s...]
    unnamed x2 -> x1, local copies, waits for them, and re-layouts: 3.62 us -> 1.72 us
    another operation x3 -> x0, other arithmetic: 1.5 us -> none
where the time goes in v2:
time: 59.5 us; the launch traced here: 59.3 us
  Pallas kernels  57.5 us (97%)
  local copies, waits for them, and re-layouts  1.72 us (3%)
    pallas_call x1, Pallas kernels, per_device(): call(latents, context, cond_vec.reshape(1, -1), ctx_vec.reshape(1, -1), s...  57.5 us
    unnamed x1, local copies, waits for them, and re-layouts  1.72 us

profile of v2, /device:TPU:0, one launch (start us, length us, event | category | flops | bytes accessed | tf_op | source)
XLA Modules:
  0.0 59.3 jit_solution(15990503140534962692)
XLA Ops:
  0.0 57.5 %shard_map.190 = bf16[80,2048]{1,0:T(8,128)(2,1)} custom-call(bf16[80,2048]{1,0:T(8,128)(2,1)} %lat_hbm.1, bf16[128,2048]{1,0:T(8,128)(2,1)} %ctx_hbm.1, f32[1,2048]{1,0:T(1,128)} %bitcast.8, f32[1,2048]{1,0:T(1,128)} %bitcast.9, bf16[256,512]{1,0:T(8,128)(2,1)} %shift_hbm.1, bf16[256,512]{1,0:T(8,128)(2,1)} %scale_hbm.1, bf16[256,512]{1,0:T(8,128)(2,1)} %mgate_hbm.1, ...), custom_call_target="tpu_custom_call" | custom-call | tf_op jit(solution)/shard_map/pallas_call | solution.py:508
  57.6 1.7 %copy.22 = bf16[80,2048]{1,0:T(8,128)(2,1)} copy(bf16[80,2048]{1,0:T(8,128)(2,1)} %shard_map.190) | data formatting | bytes 655360

commit v3 on v2

--- a/solution.py
+++ b/solution.py
@@ -279,6 +279,20 @@
 
         def left_copy(owner, s):
             return remote(part(owner, core), part(owner, core), rl_s.at[s], rl_r.at[s], (left, tp))
+
+        first_rows = half // 2 // 16 * 16
+
+        def end_right(owner):
+            at = pl.ds(pl.multiple_of(core * half, 16), first_rows)
+            return remote(
+                codes.at[owner, at, :], codes.at[owner, at, :], rr_s.at[last], rr_r.at[last], (right, tp)
+            )
+
+        def end_left(owner):
+            at = pl.ds(pl.multiple_of(core * half + first_rows, 16), half - first_rows)
+            return remote(
+                codes.at[owner, at, :], codes.at[owner, at, :], rl_s.at[last], rl_r.at[last], (left, tp)
+            )
 
         def hand_right(owner, s, c):
             return remote(part(owner, c), part(owner, c), dr_s.at[s], dr_r.at[s], (sp, partner))
@@ -344,14 +358,26 @@
             from_left = (r + n_sp - s) % n_sp
             from_right = (r + s) % n_sp
             right_copy(from_left, s).wait_recv()
-            right_copy(from_left, s + 1).start()
-            hand_right(from_left, s, core).start()
+
+            @pl.when(s < last - 1)
+            def _():
+                right_copy(from_left, s + 1).start()
+
+            @pl.when(s == last - 1)
+            def _():
+                end_right(from_left).start()
+
             left_copy(from_right, s).wait_recv()
 
             @pl.when(s < last - 1)
             def _():
                 left_copy(from_right, s + 1).start()
 
+            @pl.when(s == last - 1)
+            def _():
+                end_left(from_right).start()
+
+            hand_right(from_left, s, core).start()
             hand_left(from_right, s, core).start()
 
         def near_blocks(s):
@@ -387,7 +413,8 @@
         for x2 in others:
             attend(near, chip_at(x2), 0, middle)
         far = (r + n_sp - last) % n_sp
-        right_copy(far, last).wait_recv()
+        end_right(far).wait_recv()
+        end_left(far).wait_recv()
         hand_right(far, last, core).start()
         for x2 in others:
             attend(near, chip_at(x2), middle, pairs)
@@ -440,17 +467,19 @@
         left_copy(r, 1).wait_send()
 
         def drain(s, carry):
-            right_copy(r, s + 1).wait_send()
             hand_right(r, s, core).wait_send()
             hand_left(r, s, core).wait_send()
 
             @pl.when(s < last - 1)
             def _():
+                right_copy(r, s + 1).wait_send()
                 left_copy(r, s + 1).wait_send()
 
             return carry
 
         lax.fori_loop(1, last, drain, 0)
+        end_right(r).wait_send()
+        end_left(r).wait_send()
         hand_right(r, last, core).wait_send()
 
     def scratch():

time: 59.5 us -> 58.6 us (0.985)
  Pallas kernels: 57.5 us -> 56.6 us
    pallas_call x1, Pallas kernels: 57.5 us -> 56.6 us  [per_device(): call(latents, context, cond_vec.reshape(1, -1), ctx_vec.reshape(1, -1), s...]
where the time goes in v3:
time: 58.6 us; the launch traced here: 58.3 us
  Pallas kernels  56.6 us (97%)
  local copies, waits for them, and re-layouts  1.72 us (3%)
    pallas_call x1, Pallas kernels, per_device(): call(latents, context, cond_vec.reshape(1, -1), ctx_vec.reshape(1, -1), s...  56.6 us
    unnamed x1, local copies, waits for them, and re-layouts  1.72 us

profile of v3, /device:TPU:0, one launch (start us, length us, event | category | flops | bytes accessed | tf_op | source)
XLA Modules:
  0.0 58.3 jit_solution(6713980292732322481)
XLA Ops:
  0.0 56.6 %shard_map.190 = bf16[80,2048]{1,0:T(8,128)(2,1)} custom-call(bf16[80,2048]{1,0:T(8,128)(2,1)} %lat_hbm.1, bf16[128,2048]{1,0:T(8,128)(2,1)} %ctx_hbm.1, f32[1,2048]{1,0:T(1,128)} %bitcast.8, f32[1,2048]{1,0:T(1,128)} %bitcast.9, bf16[256,512]{1,0:T(8,128)(2,1)} %shift_hbm.1, bf16[256,512]{1,0:T(8,128)(2,1)} %scale_hbm.1, bf16[256,512]{1,0:T(8,128)(2,1)} %mgate_hbm.1, ...), custom_call_target="tpu_custom_call" | custom-call | tf_op jit(solution)/shard_map/pallas_call | solution.py:537
  56.6 1.7 %copy.22 = bf16[80,2048]{1,0:T(8,128)(2,1)} copy(bf16[80,2048]{1,0:T(8,128)(2,1)} %shard_map.190) | data formatting | bytes 655360
